TPU v7x, 32 devices: a whole 2x2x4 slice. The times are simulated.
32 devices in a mesh: sp: 8 (over z, core), tp: 4 (over y, x).
Axes of the slice: x: 2, y: 2, z: 4, core: 2. Of those that a mesh axis runs over, the one named last changes fastest.
Arguments:
- moe_input: bfloat16 [1024, 2048], P('sp', 'tp'), may hold values from -6 to 6
- cotangent: bfloat16 [1024, 2048], P('sp', 'tp'), may hold values from -6 to 6
- routes: int32 [1024, 2], P('sp'), may hold values from 0 to 7, all different within a row; in each aligned block of 128 rows (0 to 127, 128 to 255, ...) at most 40 rows name the same one
- route_weights: float32 [1024, 2], P('sp'), may hold values from 0.2 to 1
- gate_branch: bfloat16 [1024, 2560], P('sp', 'tp'), may hold values from -6 to 6
- log_decay: float32 [1024, 2560], P('sp', 'tp'), may hold values from -0.12 to 0
- states: float32 [1024, 2560], P('sp', 'tp'), may hold values from -6 to 6
- w_gate: bfloat16 [8, 2048, 2048], P('sp', None, 'tp'), may hold values from -0.125 to 0.125
- w_up: bfloat16 [8, 2048, 2048], P('sp', None, 'tp'), may hold values from -0.125 to 0.125
- w_down: bfloat16 [8, 2048, 2048], P('sp', 'tp'), may hold values from -0.125 to 0.125
- out_proj: bfloat16 [2048, 2560], P('sp', 'tp'), may hold values from -0.125 to 0.125
Outputs:
- grad_w_gate: float32 [8, 2048, 2048], P('sp', None, 'tp')
- grad_w_up: float32 [8, 2048, 2048], P('sp', None, 'tp')
- grad_w_down: float32 [8, 2048, 2048], P('sp', 'tp')
- grad_out_proj: float32 [2048, 2560], P('sp', 'tp')
- grad_gate_branch: bfloat16 [1024, 2560], P('sp', 'tp')
- grad_log_decay: bfloat16 [1024, 2560], P('sp', 'tp')
- grad_input_term: float32 [1024, 2560], P('sp', 'tp')
Inputs may be any that keep to these rules, and one draw needn't show every extreme that they name: `routes`: in the rows of one device no expert is named by more than 40 entries, and in every draw some expert is named by exactly 40 entries of one device's rows.
All inputs are finite; a program needn't handle non-finite values.
Results may differ from a plain program's by a relative error of at most 0.025.
Values may be sent and summed in bfloat16 or wider, within the bound.
No kernel may reach another device: no remote copies, remote signals or barrier semaphores. Data moves between devices by JAX's collectives and lax.ppermute only.
A program may use at most 64 MiB of HBM per device.

v0:
```python
import jax
import jax.numpy as jnp
from jax import lax
from jax.sharding import PartitionSpec as P


def carried_in(value, axis, join, neutral):
    count, mine = (lax.axis_size(axis), lax.axis_index(axis))
    pieces = jax.tree.map(lambda part: lax.all_gather(part, axis), value)
    pieces = jax.tree.map(lambda part: part[::-1], pieces)
    mine = count - 1 - mine
    subtotal = jax.tree.map(
        lambda part, zero: jnp.full_like(part, 0) + jnp.asarray(zero, part.dtype), value, neutral
    )

    def turn(position, subtotal):
        longer = join(subtotal, jax.tree.map(lambda part: part[position], pieces))
        return jax.tree.map(lambda new, old: jnp.where(position < mine, new, old), longer, subtotal)

    return lax.fori_loop(0, count - 1, turn, subtotal)


def from_behind(value, axis, steps):
    count = lax.axis_size(axis)
    leading, last = (max(0, -steps), min(count, count - steps))
    return lax.ppermute(value, axis, [(source, source + steps) for source in range(leading, last)])


def silu_parts(pre_gate):
    sigmoid_val = jax.nn.sigmoid(pre_gate)
    return (pre_gate * sigmoid_val, sigmoid_val * (1.0 + pre_gate * (1.0 - sigmoid_val)))


def combine_pair(left_pair, right_pair):
    return (left_pair[0] * right_pair[0], right_pair[0] * left_pair[1] + right_pair[1])


def compose_maps(earlier, later_map):
    return (earlier[0] * later_map[0], later_map[1] + later_map[0] * earlier[1])


def contract_rows(left_mat, right_mat):
    return lax.dot_general(
        left_mat, right_mat, (((0,), (0,)), ((), ())), preferred_element_type=jnp.float32
    )


def contract_cols(left_mat, right_mat):
    return lax.dot_general(
        left_mat, right_mat, (((1,), (1,)), ((), ())), preferred_element_type=jnp.float32
    )


def shards(
    moe_input,
    cotangent,
    routes,
    route_weights,
    gate_branch,
    log_decay,
    states,
    w_gate,
    w_up,
    w_down,
    out_proj,
):
    groups = lax.axis_size("sp")
    tok_rows, picks = routes.shape
    col_width = moe_input.shape[1]
    model_width = col_width * lax.axis_size("tp")
    room = tok_rows * picks * 5 // (4 * groups)
    flat_routes = routes.reshape(-1)
    onehot = (flat_routes[:, None] == jnp.arange(groups, dtype=jnp.int32)[None, :]).astype(
        jnp.int32
    )
    before = jnp.cumsum(onehot, axis=0) - onehot
    slot_index = jnp.sum(before * onehot, axis=1)
    target = flat_routes * room + slot_index
    owners = jnp.arange(tok_rows * picks, dtype=jnp.int32) // picks
    source = jnp.zeros((groups * room,), jnp.int32).at[target].set(owners)
    live_slot = jnp.zeros((groups * room,), jnp.bool_).at[target].set(True)
    slot_weight = jnp.zeros((groups * room,), jnp.float32).at[target].set(route_weights.reshape(-1))
    send_data = jnp.where(live_slot[:, None], moe_input[source], jnp.zeros((), jnp.bfloat16))
    send_cot = (slot_weight[:, None] * cotangent[source].astype(jnp.float32)).astype(jnp.bfloat16)
    part_rows, part_cot = (
        lax.all_to_all(
            send_data.reshape(groups, room, col_width),
            "sp",
            split_axis=0,
            concat_axis=0,
            tiled=True,
        ),
        lax.all_to_all(
            send_cot.reshape(groups, room, col_width), "sp", split_axis=0, concat_axis=0, tiled=True
        ),
    )
    rows_in, cot_in = (
        lax.all_gather(part_rows, "tp", axis=2, tiled=True),
        lax.all_gather(part_cot, "tp", axis=2, tiled=True),
    )
    row_data = rows_in.reshape(groups * room, model_width)
    scaled = cot_in.reshape(groups * room, model_width)
    gate_w = w_gate[0]
    up_w = w_up[0]
    down_w = w_down[0]
    pre_gate = jnp.dot(row_data, gate_w, preferred_element_type=jnp.float32)
    pre_up = jnp.dot(row_data, up_w, preferred_element_type=jnp.float32)
    active, slope = silu_parts(pre_gate)
    hidden = (active * pre_up).astype(jnp.bfloat16)
    grad_down = contract_rows(hidden, scaled)
    grad_hidden = contract_cols(scaled, down_w)
    grad_pre_gate = (grad_hidden * pre_up * slope).astype(jnp.bfloat16)
    grad_pre_up = (grad_hidden * active).astype(jnp.bfloat16)
    grad_gate_w = contract_rows(row_data, grad_pre_gate)
    grad_up_w = contract_rows(row_data, grad_pre_up)
    joined_grads = jnp.concatenate([grad_pre_gate, grad_pre_up], axis=1)
    joined_weights = jnp.concatenate([gate_w, up_w], axis=1)
    entry_terms = contract_cols(joined_grads, joined_weights)
    summed = lax.psum_scatter(
        entry_terms.reshape(groups, room, model_width).astype(jnp.bfloat16),
        "tp",
        scatter_dimension=2,
        tiled=True,
    )
    returned = lax.all_to_all(summed, "sp", split_axis=0, concat_axis=0, tiled=True)
    back_rows = returned.reshape(groups * room, col_width)[target].astype(jnp.float32)
    grad_cols = (
        jnp.sum(back_rows.reshape(tok_rows, picks, col_width), axis=1)
        + cotangent.astype(jnp.float32)
    ).astype(jnp.bfloat16)
    grad_tokens = lax.all_gather(grad_cols, "tp", axis=1, tiled=True)
    active_gate, pullback = jax.vjp(jax.nn.gelu, gate_branch.astype(jnp.float32))
    mixed_in = (active_gate * states).astype(jnp.bfloat16)
    piece_cols = grad_tokens
    grad_out_proj = lax.psum_scatter(
        contract_rows(piece_cols, mixed_in).astype(jnp.bfloat16),
        "sp",
        scatter_dimension=0,
        tiled=True,
    ).astype(jnp.float32)
    piece_cols = grad_tokens
    grad_mixed = jnp.dot(
        piece_cols,
        lax.all_gather(out_proj, "sp", axis=0, tiled=True),
        preferred_element_type=jnp.float32,
    )
    grad_gate_branch = pullback(grad_mixed * states)[0].astype(jnp.bfloat16)
    grad_state = grad_mixed * active_gate
    decays = jnp.exp(log_decay)
    next_decay = jnp.concatenate([decays[1:], jnp.ones_like(decays[:1])], axis=0)
    span_flip, local_flip = lax.associative_scan(
        combine_pair, (jnp.flip(next_decay, 0), jnp.flip(grad_state, 0))
    )
    span_decay = jnp.flip(span_flip, 0)
    local_grad = jnp.flip(local_flip, 0)
    whole_decay = span_decay[0] * decays[0]
    entry_term = decays[0] * local_grad[0]
    carried = carried_in(
        (whole_decay, entry_term),
        "sp",
        compose_maps,
        (jnp.ones_like(whole_decay), jnp.zeros_like(entry_term)),
    )
    grad_input_term = local_grad + span_decay * carried[1][None, :]
    earlier_state = from_behind(states[-1:], "sp", 1)
    prev_states = jnp.concatenate([earlier_state, states[:-1]], axis=0)
    grad_log_decay = (grad_input_term * decays * prev_states).astype(jnp.bfloat16)
    return (
        grad_gate_w[None],
        grad_up_w[None],
        grad_down[None],
        grad_out_proj,
        grad_gate_branch,
        grad_log_decay,
        grad_input_term,
    )


def solution(mesh):
    return jax.shard_map(
        shards,
        mesh=mesh,
        in_specs=(
            P("sp", "tp"),
            P("sp", "tp"),
            P("sp", None),
            P("sp", None),
            P("sp", "tp"),
            P("sp", "tp"),
            P("sp", "tp"),
            P("sp", None, "tp"),
            P("sp", None, "tp"),
            P("sp", "tp", None),
            P("sp", "tp"),
        ),
        out_specs=(
            P("sp", None, "tp"),
            P("sp", None, "tp"),
            P("sp", "tp", None),
            P("sp", "tp"),
            P("sp", "tp"),
            P("sp", "tp"),
            P("sp", "tp"),
        ),
        check_vma=False,
    )
```

profile of v0, /device:TPU:0, one launch (start us, length us, event | category | flops | bytes accessed | tf_op | source)
XLA Modules:
  0.0 252.5 jit_solution(4397792106868432355)
XLA Ops:
  16.4 17.4 %all_to_all.15 = bf16[8,40,512]{2,1,0:T(8,128)(2,1)} all-to-all(bf16[8,40,512]{2,1,0:T(8,128)(2,1)S(1)} %broadcast_select_fusion), channel_id=1, replica_groups=mesh['sp'=8,'tp'=4] {'sp'}, dimensions={0} | all-to-all | bytes 655360 | tf_op jit(solution)/shard_map/all_to_all | solution.py:86
  37.8 14.2 %all_to_all.16 = bf16[8,40,512]{2,1,0:T(8,128)(2,1)} all-to-all(bf16[8,40,512]{2,1,0:T(8,128)(2,1)S(1)} %fusion.12), channel_id=1, replica_groups=mesh['sp'=8,'tp'=4] {'sp'}, dimensions={0} | all-to-all | bytes 655360 | tf_op jit(solution)/shard_map/all_to_all | solution.py:93
  52.0 9.4 %all-gather.6.cloned.1.call-done = bf16[8,40,2048]{2,1,0:T(8,128)(2,1)} async-done(((bf16[8,40,512]{2,1,0:T(8,128)(2,1)}), bf16[8,40,2048]{2,1,0:T(8,128)(2,1)}) %all-gather.6.cloned.1.call-update) | async-done | bytes 1310736 | tf_op jit(solution)/shard_map/all_gather | solution.py:98
  61.4 3.8 %fusion.51 = f32[320,512]{1,0:T(8,128)} fusion(bf16[320,2048]{1,0:T(8,128)(2,1)} %bitcast.60, bf16[1,2048,512]{2,1,0:T(8,128)(2,1)} %param.20), kind=kOutput, calls=%fused_computation.129 | convolution fusion | flops 671088640 | bytes 4063232 | tf_op jit(solution)/shard_map/dot_general | solution.py:106
  66.9 24.9 %all-gather.8.cloned.1.call-done = bf16[8,40,2048]{2,1,0:T(8,128)(2,1)} async-done(((bf16[8,40,512]{2,1,0:T(8,128)(2,1)}), bf16[8,40,2048]{2,1,0:T(8,128)(2,1)}) %all-gather.8.cloned.1.call-update) | async-done | bytes 1310736 | tf_op jit(solution)/shard_map/all_gather | solution.py:99
  91.8 2.9 %multiply_convert_fusion.1 = (bf16[320,512]{1,0:T(8,128)(2,1)S(1)}, bf16[320,512]{1,0:T(8,128)(2,1)S(1)}) fusion(f32[320,512]{1,0:T(8,128)} %fusion.51, f32[320,512]{1,0:T(8,128)} %fusion.53, bf16[320,2048]{1,0:T(8,128)(2,1)} %bitcast.77, bf16[1,512,2048]{2,1,0:T(8,128)(2,1)S(1)} %copy-done), kind=kOutput, calls=%fused_computation.31 | convolution fusion | flops 673218560 | bytes 5373952 | tf_op jit(solution)/shard_map/dot_general | solution.py:49
  94.8 2.6 %fusion.4 = bf16[320,2048]{1,0:T(8,128)(2,1)} fusion(bf16[2048,512]{1,0:T(8,128)(2,1)S(1)} %bitcast.76, bf16[2048,512]{1,0:T(8,128)(2,1)S(1)} %bitcast.75, bf16[320,512]{1,0:T(8,128)(2,1)S(1)} %get-tuple-element.134, bf16[320,512]{1,0:T(8,128)(2,1)S(1)} %get-tuple-element.135), kind=kOutput, calls=%fused_computation.17 | convolution fusion | flops 1352531968 | bytes 6160384 | tf_op jit(solution)/shard_map/dot_general | solution.py:49
  109.0 2.9 %slice.259 = f32[64,640]{1,0:T(8,128)} reverse(f32[64,640]{1,0:T(8,128)} %slice.258), dimensions={0} | reverse | bytes 327680 | tf_op jit(solution)/shard_map/slice | solution.py:151
  112.0 3.0 %slice.250 = f32[63,640]{1,0:T(8,128)} reverse(f32[63,640]{1,0:T(8,128)} %slice.249), dimensions={0} | reverse | bytes 322560 | tf_op jit(solution)/shard_map/slice | solution.py:151
  114.9 2.9 %slice.252 = f32[64,640]{1,0:T(8,128)} reverse(f32[64,640]{1,0:T(8,128)} %slice.251), dimensions={0} | reverse | bytes 327680 | tf_op jit(solution)/shard_map/slice | solution.py:151
  117.9 4.3 %convolution_bitcast_fusion.2 = f32[1,2048,512]{2,1,0:T(8,128)} fusion(bf16[320,2048]{1,0:T(8,128)(2,1)S(1)} %bitcast.63, bf16[320,512]{1,0:T(8,128)(2,1)} %copy-done.11), kind=kOutput, calls=%fused_computation.15 | convolution fusion | flops 671088640 | bytes 5832704 | tf_op jit(solution)/shard_map/dot_general | solution.py:43
  122.2 4.9 %reduce-scatter.3.cloned.1.call-done = bf16[8,40,512]{2,1,0:T(8,128)(2,1)} async-done(((bf16[8,40,2048]{2,1,0:T(8,128)(2,1)}), bf16[8,40,512]{2,1,0:T(8,128)(2,1)}) %reduce-scatter.3.cloned.1.call-update) | async-done | bytes 327696 | tf_op jit(solution)/shard_map/reduce_scatter | solution.py:119
  127.1 4.6 %all-to-all-start.2 = ((bf16[8,40,512]{2,1,0:T(8,128)(2,1)}), bf16[8,40,512]{2,1,0:T(8,128)(2,1)S(1)}, u32[]{:S(2)}, u32[]{:S(2)}) async-start(bf16[8,40,512]{2,1,0:T(8,128)(2,1)} %reduce-scatter.3.cloned.1.call-done), calls=%async_computation.3 | async-start | bytes 655360 | tf_op jit(solution)/shard_map/all_to_all | solution.py:125
  132.0 4.8 %convolution_bitcast_fusion.1 = f32[1,2048,512]{2,1,0:T(8,128)} fusion(bf16[320,2048]{1,0:T(8,128)(2,1)} %bitcast.61, bf16[320,512]{1,0:T(8,128)(2,1)} %copy-done.10), kind=kOutput, calls=%fused_computation.14 | convolution fusion | flops 671088640 | bytes 5832704 | tf_op jit(solution)/shard_map/dot_general | solution.py:43
  136.8 3.4 %convolution_bitcast_fusion = f32[1,512,2048]{2,1,0:T(8,128)} fusion(bf16[320,2048]{1,0:T(8,128)(2,1)S(1)} %bitcast.78, f32[320,512]{1,0:T(8,128)S(1)} %copy-done.24, f32[320,512]{1,0:T(8,128)S(1)} %copy-done.23), kind=kOutput, calls=%fused_computation.13 | convolution fusion | flops 672071680 | bytes 6815744 | tf_op jit(solution)/shard_map/dot_general | solution.py:43
  140.2 2.7 %all-to-all-done.2 = bf16[8,40,512]{2,1,0:T(8,128)(2,1)S(1)} async-done(((bf16[8,40,512]{2,1,0:T(8,128)(2,1)}), bf16[8,40,512]{2,1,0:T(8,128)(2,1)S(1)}, u32[]{:S(2)}, u32[]{:S(2)}) %all-to-all-start.2) | async-done | bytes 327712 | tf_op jit(solution)/shard_map/all_to_all | solution.py:125
  145.0 10.4 %all_gather.22 = bf16[128,2048]{1,0:T(8,128)(2,1)S(1)} all-gather(bf16[128,512]{1,0:T(8,128)(2,1)S(1)} %add_convert_fusion), channel_id=1, replica_groups=mesh['sp'=8,'tp'=4] {'tp'}, dimensions={1}, use_global_device_ids=true | all-gather | bytes 655360 | tf_op jit(solution)/shard_map/all_gather | solution.py:131
  155.3 3.1 %fusion.24 = (f32[128,640]{1,0:T(8,128)S(1)}, bf16[128,640]{1,0:T(8,128)(2,1)}) fusion(bf16[128,640]{1,0:T(8,128)(2,1)} %param.17, f32[128,640]{1,0:T(8,128)S(1)} %copy-done.4, bf16[128,2048]{1,0:T(8,128)(2,1)S(1)} %all_gather.22, bf16[2048,640]{1,0:T(8,128)(2,1)} %all-gather.10.cloned.1.call-done), kind=kOutput, calls=%fused_computation.50 | convolution fusion | flops 337510400 | bytes 4128768 | tf_op jit(solution)/shard_map/dot_general | solution.py:142
  159.9 2.9 %slice.254 = f32[64,640]{1,0:T(8,128)} reverse(f32[64,640]{1,0:T(8,128)} %slice.253), dimensions={0} | reverse | bytes 327680 | tf_op jit(solution)/shard_map/slice | solution.py:151
  162.9 2.9 %slice.256 = f32[64,640]{1,0:T(8,128)} reverse(f32[64,640]{1,0:T(8,128)} %slice.255), dimensions={0} | reverse | bytes 327680 | tf_op jit(solution)/shard_map/slice | solution.py:151
  183.2 3.3 %convolution_convert_fusion = bf16[2048,640]{1,0:T(8,128)(2,1)} fusion(bf16[128,2048]{1,0:T(8,128)(2,1)S(1)} %all_gather.22, f32[128,640]{1,0:T(8,128)S(1)} %copy-done.4, bf16[128,640]{1,0:T(8,128)(2,1)} %param.17), kind=kOutput, calls=%fused_computation.16 | convolution fusion | flops 337756160 | bytes 3637248 | tf_op jit(solution)/shard_map/dot_general | solution.py:43
  205.8 14.0 %all-gather.1 = f32[8,1,640]{2,1,0:T(1,128)S(1)} all-gather(f32[1,1,640]{2,1,0:T(1,128)S(1)} %get-tuple-element.138), channel_id=1, replica_groups=mesh['sp'=8,'tp'=4] {'sp'}, dimensions={0}, use_global_device_ids=true | all-gather | bytes 23040 | tf_op jit(solution)/shard_map/all_gather | solution.py:9
  219.8 13.9 %all-gather = f32[8,1,640]{2,1,0:T(1,128)S(1)} all-gather(f32[1,1,640]{2,1,0:T(1,128)S(1)} %get-tuple-element.139), channel_id=1, replica_groups=mesh['sp'=8,'tp'=4] {'sp'}, dimensions={0}, use_global_device_ids=true | all-gather | bytes 23040 | tf_op jit(solution)/shard_map/all_gather | solution.py:9
  236.9 2.5 %rev.16 = f32[128,640]{1,0:T(8,128)S(1)} reverse(f32[128,640]{1,0:T(8,128)} %add.255), dimensions={0} | reverse | bytes 655360 | tf_op jit(solution)/shard_map/jit(_flip)/rev | solution.py:154
  (231 shorter events, 75.1 us)
Async XLA Ops:
  8.0 83.8 %copy-start = (bf16[1,512,2048]{2,1,0:T(8,128)(2,1)S(1)}, bf16[1,512,2048]{2,1,0:T(8,128)(2,1)}, u32[]{:S(2)}) copy-start(bf16[1,512,2048]{2,1,0:T(8,128)(2,1)} %param.22) | copy-start | bytes 6291460
  8.0 6.2 %copy-start.2 = (bf16[128,512]{1,0:T(8,128)(2,1)S(1)}, bf16[128,512]{1,0:T(8,128)(2,1)}, u32[]{:S(2)}) copy-start(bf16[128,512]{1,0:T(8,128)(2,1)} %param.13) | copy-start | bytes 393220
  8.0 53.4 %all-gather.6.cloned.1.call-start = ((), (), s32[]{:S(2)}) async-start(), calls=%async_computation.5 | async-start | bytes 1638400 | tf_op jit(solution)/shard_map/all_gather | solution.py:98
  14.2 19.6 %copy-start.18 = (f32[128,2]{0,1:T(2,128)S(1)}, f32[128,2]{0,1:T(2,128)}, u32[]{:S(2)}) copy-start(f32[128,2]{0,1:T(2,128)} %param.16) | copy-start | bytes 3076
  14.2 21.4 %copy-start.1 = (bf16[128,512]{1,0:T(8,128)(2,1)S(1)}, bf16[128,512]{1,0:T(8,128)(2,1)}, u32[]{:S(2)}) copy-start(bf16[128,512]{1,0:T(8,128)(2,1)} %param.14) | copy-start | bytes 393220
  33.8 58.0 %all-gather.8.cloned.1.call-start = ((), (), s32[]{:S(2)}) async-start(), calls=%async_computation.6 | async-start | bytes 1638400 | tf_op jit(solution)/shard_map/all_gather | solution.py:99
  52.0 75.1 %reduce-scatter.3.cloned.1.call-start = ((), (), s32[]{:S(2)}) async-start(), calls=%async_computation.7 | async-start | bytes 1638400 | tf_op jit(solution)/shard_map/reduce_scatter | solution.py:119
  61.4 3.8 %copy-start.3 = (bf16[8,40,2048]{2,1,0:T(8,128)(2,1)S(1)}, bf16[8,40,2048]{2,1,0:T(8,128)(2,1)}, u32[]{:S(2)}) copy-start(bf16[8,40,2048]{2,1,0:T(8,128)(2,1)} %all-gather.6.cloned.1.call-done) | copy-start | bytes 3932164
  61.4 3.8 %copy-start.20 = (bf16[1,2048,512]{2,1,0:T(8,128)(2,1)S(1)}, bf16[1,2048,512]{2,1,0:T(8,128)(2,1)}, u32[]{:S(2)}) copy-start(bf16[1,2048,512]{2,1,0:T(8,128)(2,1)} %param.21) | copy-start | bytes 6291460
  91.8 2.9 %copy-start.19 = (bf16[1,2048,512]{2,1,0:T(8,128)(2,1)S(1)}, bf16[1,2048,512]{2,1,0:T(8,128)(2,1)}, u32[]{:S(2)}) copy-start(bf16[1,2048,512]{2,1,0:T(8,128)(2,1)} %param.20) | copy-start | bytes 6291460
  91.8 3.0 %copy-start.21 = (bf16[1,2048,512]{2,1,0:T(8,128)(2,1)S(1)}, bf16[1,2048,512]{2,1,0:T(8,128)(2,1)}, u32[]{:S(2)}) copy-start(bf16[1,2048,512]{2,1,0:T(8,128)(2,1)} %param.21) | copy-start | bytes 6291460
  97.5 57.9 %all-gather.10.cloned.1.call-start = ((), (), s32[]{:S(2)}) async-start(), calls=%async_computation.9 | async-start | bytes 2949120 | tf_op jit(solution)/shard_map/all_gather | solution.py:144
  99.4 142.6 %collective-permute-start = (f32[1,640]{1,0:T(1,128)}, f32[1,640]{1,0:T(1,128)}, u32[]{:S(2)}, u32[]{:S(2)}) collective-permute-start(f32[1,640]{1,0:T(1,128)} %slice.320), channel_id=1, source_target_pairs={{0,4},{4,8},{8,12},{12,16},{16,20},{20,24},{24,28},{1,5},{5,9},{9,... | collective-permute-start | bytes 7688 | tf_op jit(solution)/shard_map/ppermute | solution.py:26
  127.1 15.7 %all-to-all-start.2 = ((bf16[8,40,512]{2,1,0:T(8,128)(2,1)}), bf16[8,40,512]{2,1,0:T(8,128)(2,1)S(1)}, u32[]{:S(2)}, u32[]{:S(2)}) async-start(bf16[8,40,512]{2,1,0:T(8,128)(2,1)} %reduce-scatter.3.cloned.1.call-done), calls=%async_computation.3 | async-start | bytes 655360 | tf_op jit(solution)/shard_map/all_to_all | solution.py:125
  131.7 5.1 %copy-start.23 = (f32[320,512]{1,0:T(8,128)S(1)}, f32[320,512]{1,0:T(8,128)}, u32[]{:S(2)}) copy-start(f32[320,512]{1,0:T(8,128)} %fusion.51) | copy-start | bytes 1966084
  131.7 111.8 %reduce-scatter.5.cloned.1.call-start = ((), (), s32[]{:S(2)}) async-start(), calls=%async_computation.8 | async-start | bytes 2949120 | tf_op jit(solution)/shard_map/reduce_scatter | solution.py:135
  131.9 4.8 %copy-start.22 = (bf16[8,40,2048]{2,1,0:T(8,128)(2,1)S(1)}, bf16[8,40,2048]{2,1,0:T(8,128)(2,1)}, u32[]{:S(2)}) copy-start(bf16[8,40,2048]{2,1,0:T(8,128)(2,1)} %all-gather.8.cloned.1.call-done) | copy-start | bytes 3932164
  132.0 4.8 %copy-start.24 = (f32[320,512]{1,0:T(8,128)S(1)}, f32[320,512]{1,0:T(8,128)}, u32[]{:S(2)}) copy-start(f32[320,512]{1,0:T(8,128)} %fusion.53) | copy-start | bytes 1966084
  142.8 12.5 %copy-start.4 = (f32[128,640]{1,0:T(8,128)S(1)}, f32[128,640]{1,0:T(8,128)}, u32[]{:S(2)}) copy-start(f32[128,640]{1,0:T(8,128)} %param.19) | copy-start | bytes 983044
  158.4 4.4 %copy-start.7 = (f32[128,640]{1,0:T(8,128)}, f32[128,640]{1,0:T(8,128)S(1)}, u32[]{:S(2)}) copy-start(f32[128,640]{1,0:T(8,128)S(1)} %get-tuple-element.136) | copy-start | bytes 983044
  189.9 7.5 %copy-start.12 = (f32[31,640]{1,0:T(8,128)S(1)}, f32[31,640]{1,0:T(8,128)}, u32[]{:S(2)}) copy-start(f32[31,640]{1,0:T(8,128)} %slice.301) | copy-start | bytes 238084
  194.6 3.5 %copy-start.17 = (f32[1,640]{1,0:T(1,128)S(1)}, f32[1,640]{1,0:T(1,128)}, u32[]{:S(2)}) copy-start(f32[1,640]{1,0:T(1,128)} %slice.353) | copy-start | bytes 7684
  196.0 5.5 %copy-start.9 = (f32[63,640]{1,0:T(8,128)S(1)}, f32[63,640]{1,0:T(8,128)}, u32[]{:S(2)}) copy-start(f32[63,640]{1,0:T(8,128)} %slice.250) | copy-start | bytes 483844
  236.1 5.9 %copy-start.6 = (f32[128,640]{1,0:T(8,128)S(1)}, f32[128,640]{1,0:T(8,128)}, u32[]{:S(2)}) copy-start(f32[128,640]{1,0:T(8,128)} %param.18) | copy-start | bytes 983044
  (8 other events, 10.4 us)
Sparse Core Ops, SparseCore 0:
  33.9 27.4 all-gather.5
  63.3 28.5 all-gather.7
  97.6 29.4 reduce-scatter.2
Sparse Core Ops, SparseCore 1:
  99.6 33.5 all-gather.9
  186.6 35.5 reduce-scatter.4
where the time goes:
time: 256 us; the launch traced here: 252 us
  blocking collectives  69.8 us (27%)
  local copies, waits for them, and re-layouts  68.4 us (27%)
  waiting for transfers between devices  42.5 us (17%)
  matrix products  29.8 us (12%)
  other arithmetic  18.7 us (7%)
  between operations  15.9 us (6%)
  starting transfers between devices  7.14 us (3%)
    slice x49, local copies, waits for them, and re-layouts, shards(): lax.associative_scan(combine_pair, (jnp.flip(next_decay, 0), jnp.flip(gra...  40.8 us
    all_gather x2, blocking collectives, carried_in(): pieces = jax.tree.map(lambda part: lax.all_gather(part, axis), value)  27.9 us
    all_gather x1, waiting for transfers between devices, shards(): lax.all_gather(part_cot, 'tp', axis=2, tiled=True)  24.9 us
    all_to_all x1, blocking collectives, shards(): lax.all_to_all(send_data.reshape(groups, room, col_width), 'sp', split_ax...  17.4 us
    dot_general x4, matrix products, contract_rows(): lax.dot_general(left_mat, right_mat, (((0,), (0,)), ((), ())), preferred_...  15.8 us
    all_to_all x1, blocking collectives, shards(): lax.all_to_all(send_cot.reshape(groups, room, col_width), 'sp', split_axi...  14.2 us
    all_gather x1, blocking collectives, shards(): grad_tokens = lax.all_gather(grad_cols, 'tp', axis=1, tiled=True)  10.4 us
    all_gather x1, waiting for transfers between devices, shards(): lax.all_gather(part_rows, 'tp', axis=2, tiled=True)  9.4 us
  transfers between devices with their start and end apart: 7, of which 4 were waited for; matrix products, arithmetic and copies ran while one was open for 40% of the time, Pallas kernels for 0%

commit v1 on v0

v1 whole, which is shorter than its diff:
```python
import functools

import jax
import jax.numpy as jnp
from jax import lax
from jax.experimental import pallas as pl
from jax.experimental.pallas import tpu as pltpu
from jax.sharding import PartitionSpec as P


F32 = jnp.float32
BF16 = jnp.bfloat16


def contract_rows(left_mat, right_mat):
    return lax.dot_general(
        left_mat, right_mat, (((0,), (0,)), ((), ())), preferred_element_type=F32
    )


def contract_cols(left_mat, right_mat):
    return lax.dot_general(
        left_mat, right_mat, (((1,), (1,)), ((), ())), preferred_element_type=F32
    )


def swap(value, axis, bits):
    count = lax.axis_size(axis)
    return lax.ppermute(value, axis, [(i, i ^ bits) for i in range(count)])


def vmem_specs(count):
    return [pl.BlockSpec(memory_space=pltpu.VMEM)] * count


def room_for(mebibytes):
    return pltpu.CompilerParams(vmem_limit_bytes=mebibytes * 1024 * 1024)


def kept(value):
    return pltpu.with_memory_space_constraint(value, pltpu.VMEM)


def kept_all(values):
    return [kept(value) for value in values]


def slots_body(groups, room, me_ref, routes_ref, weights_ref, x_ref, c_ref, *outs):
    picks, rows = routes_ref.shape
    chips = groups // 2
    relative = routes_ref[...] ^ me_ref[0]
    expert = lax.broadcasted_iota(jnp.int32, (groups, rows), 0)
    hits = [expert == relative[k : k + 1] for k in range(picks)]
    total = sum(hit.astype(F32) for hit in hits)
    earlier = lax.broadcasted_iota(jnp.int32, (rows, rows), 0) < lax.broadcasted_iota(
        jnp.int32, (rows, rows), 1
    )
    before = jnp.dot(
        total.astype(BF16), earlier.astype(F32).astype(BF16), preferred_element_type=F32
    )
    place = (expert * room).astype(F32) + before
    slot = lax.broadcasted_iota(jnp.int32, (groups * room, rows), 0)
    taken = jnp.zeros((groups * room, rows), F32)
    weight = jnp.zeros((groups * room, rows), F32)
    for k in range(picks):
        target = jnp.sum(jnp.where(hits[k], place, 0.0), axis=0, keepdims=True)
        here = slot == target.astype(jnp.int32)
        taken = jnp.where(here, 1.0, taken)
        weight = jnp.where(here, weights_ref[k : k + 1], weight)
    chosen = taken.astype(BF16)
    slot_weight = jnp.sum(weight, axis=1, keepdims=True)
    data = jnp.dot(chosen, x_ref[...], preferred_element_type=F32).astype(BF16)
    cot = (slot_weight * jnp.dot(chosen, c_ref[...], preferred_element_type=F32)).astype(BF16)
    for k in range(chips):
        outs[k][...] = data[2 * k * room : 2 * (k + 1) * room]
        outs[chips + k][...] = cot[2 * k * room : 2 * (k + 1) * room]
    outs[2 * chips][...] = chosen


def slots(me, routes, weights, x, c, groups, room):
    rows, width = x.shape
    chips = groups // 2
    piece = pltpu.VMEM((2 * room, width), BF16)
    out = pl.pallas_call(
        functools.partial(slots_body, groups, room),
        out_shape=[piece] * (2 * chips) + [pltpu.VMEM((groups * room, rows), BF16)],
        in_specs=[pl.BlockSpec(memory_space=pltpu.SMEM)] + vmem_specs(4),
        out_specs=vmem_specs(2 * chips + 1),
        compiler_params=room_for(8),
        name="slots",
    )(me, *[pltpu.with_memory_space_constraint(v, pltpu.HBM) for v in (routes, weights, x, c)])
    return out[:chips], out[chips : 2 * chips], out[2 * chips]


def forward_body(parts, order_ref, *refs):
    xs, (gate_w, up_w, pre_gate, pre_up) = refs[:parts], refs[parts:]
    width = xs[0].shape[1]
    for k in range(parts):
        at = pl.ds(pl.multiple_of(order_ref[k] * width, width), width)
        x = xs[k][...]
        gate = jnp.dot(x, gate_w[0, at, :], preferred_element_type=F32)
        up = jnp.dot(x, up_w[0, at, :], preferred_element_type=F32)
        if k == 0:
            pre_gate[...] = gate
            pre_up[...] = up
        else:
            pre_gate[...] += gate
            pre_up[...] += up


def forward(order, xs, w_gate, w_up):
    parts = len(xs)
    rows = xs[0].shape[0]
    hid = w_gate.shape[2]
    return pl.pallas_call(
        functools.partial(forward_body, parts),
        out_shape=[pltpu.VMEM((rows, hid), F32)] * 2,
        in_specs=[pl.BlockSpec(memory_space=pltpu.SMEM)] + vmem_specs(parts + 2),
        out_specs=vmem_specs(2),
        compiler_params=room_for(6),
        name="expert_forward",
    )(order, *kept_all([*xs, w_gate, w_up]))


def backward_body(parts, order_ref, *refs):
    cs, refs = refs[:parts], refs[parts:]
    down_w, gate_w, up_w, pre_gate, pre_up, hidden, grad_gate, grad_up = refs[:8]
    terms, total = refs[8 : 8 + parts], refs[8 + parts]
    width = cs[0].shape[1]
    spots = [pl.ds(pl.multiple_of(order_ref[k] * width, width), width) for k in range(parts)]
    for k in range(parts):
        part = contract_cols(cs[k][...], down_w[0, :, spots[k]])
        if k == 0:
            total[...] = part
        else:
            total[...] += part
    grad_hidden = total[...]
    gate, up = pre_gate[...], pre_up[...]
    sig = jax.nn.sigmoid(gate)
    active = gate * sig
    slope = sig * (1.0 + gate * (1.0 - sig))
    hidden[...] = (active * up).astype(BF16)
    grad_gate[...] = (grad_hidden * up * slope).astype(BF16)
    grad_up[...] = (grad_hidden * active).astype(BF16)
    for k in range(parts):
        term = contract_cols(grad_gate[...], gate_w[0, spots[k], :])
        term += contract_cols(grad_up[...], up_w[0, spots[k], :])
        terms[k][...] = term.astype(BF16)


def backward(order, cs, w_down, w_gate, w_up, pre_gate, pre_up):
    parts = len(cs)
    rows, width = cs[0].shape
    hid = w_gate.shape[2]
    out = pl.pallas_call(
        functools.partial(backward_body, parts),
        out_shape=[pltpu.VMEM((rows, hid), BF16)] * 3 + [pltpu.VMEM((rows, width), BF16)] * parts,
        in_specs=[pl.BlockSpec(memory_space=pltpu.SMEM)] + vmem_specs(parts + 5),
        out_specs=vmem_specs(3 + parts),
        scratch_shapes=[pltpu.VMEM((rows, hid), F32)],
        compiler_params=room_for(8),
        name="expert_backward",
    )(order, *kept_all([*cs, w_down, w_gate, w_up, pre_gate, pre_up]))
    return out[0], out[1], out[2], out[3:]


def weights_body(parts, order_ref, *refs):
    xs, cs, refs = refs[:parts], refs[parts : 2 * parts], refs[2 * parts :]
    hidden, grad_gate, grad_up, out_gate, out_up, out_down = refs
    step = pl.program_id(0)
    for k in range(parts):

        @pl.when(step == k)
        def _():
            x = xs[k][...]
            out_gate[0] = contract_rows(x, grad_gate[...])
            out_up[0] = contract_rows(x, grad_up[...])
            out_down[0] = contract_rows(hidden[...], cs[k][...])


def weight_grads(order, xs, cs, hidden, grad_gate, grad_up):
    parts = len(xs)
    _, width = xs[0].shape
    hid = hidden.shape[1]
    model = width * parts
    wide = pl.BlockSpec((1, width, hid), lambda i, o: (0, o[i], 0))
    down = pl.BlockSpec((1, hid, width), lambda i, o: (0, 0, o[i]))
    return pl.pallas_call(
        functools.partial(weights_body, parts),
        out_shape=[jax.ShapeDtypeStruct((1, model, hid), F32)] * 2
        + [jax.ShapeDtypeStruct((1, hid, model), F32)],
        grid_spec=pltpu.PrefetchScalarGridSpec(
            num_scalar_prefetch=1,
            grid=(parts,),
            in_specs=vmem_specs(2 * parts + 3),
            out_specs=[wide, wide, down],
        ),
        compiler_params=room_for(14),
        name="weight_grads",
    )(order, *kept_all([*xs, *cs, hidden, grad_gate, grad_up]))


def combine_body(count, chosen_ref, cot_ref, *refs):
    backs, out = refs[:count], refs[count]
    piece = backs[0].shape[0]
    total = cot_ref[...].astype(F32)
    for k in range(count):
        total += contract_rows(chosen_ref[k * piece : (k + 1) * piece], backs[k][...])
    out[...] = total.astype(BF16)


def combine(chosen, cot, backs):
    return pl.pallas_call(
        functools.partial(combine_body, len(backs)),
        out_shape=pltpu.VMEM(cot.shape, BF16),
        in_specs=vmem_specs(2 + len(backs)),
        out_specs=vmem_specs(1)[0],
        compiler_params=room_for(6),
        name="combine",
    )(*kept_all([chosen, cot, *backs]))


def gates_body(gate_ref, states_ref, active_ref, pull_ref, mixed_ref):
    gate = gate_ref[...].astype(F32)
    states = states_ref[...]
    coef = 0.7978845608028654
    inner = jnp.tanh(coef * (gate + 0.044715 * gate * gate * gate))
    half = 0.5 * (1.0 + inner)
    active = gate * half
    slope = half + 0.5 * gate * (1.0 - inner * inner) * coef * (
        1.0 + 3.0 * 0.044715 * gate * gate
    )
    active_ref[...] = active
    pull_ref[...] = states * slope
    mixed_ref[...] = (active * states).astype(BF16)


def gates(gate_branch, states):
    full = jax.ShapeDtypeStruct(states.shape, F32)
    return pl.pallas_call(
        gates_body,
        out_shape=[full, full, pltpu.VMEM(states.shape, BF16)],
        in_specs=vmem_specs(2),
        out_specs=vmem_specs(3),
        compiler_params=room_for(8),
        name="gates",
    )(gate_branch, states)


def recur_body(me_ref, tokens_ref, own_ref, other_ref, active_ref, pull_ref, log_ref,
               gate_out, local_out, span_out, edge_out):
    chips, rows, width = tokens_ref.shape
    half = width // 2
    first = (me_ref[0] & 1) == 0
    chip = me_ref[0] // 2
    mixed = jnp.zeros((rows, own_ref.shape[2]), F32)
    for k in range(chips):
        block = tokens_ref[chip ^ k]
        left, right = block[:, :half], block[:, half:]
        mine = jnp.where(first, left, right)
        theirs = jnp.where(first, right, left)
        mixed += jnp.dot(mine, own_ref[k, :half], preferred_element_type=F32)
        mixed += jnp.dot(theirs, other_ref[k, :half], preferred_element_type=F32)
    gate_out[...] = (mixed * pull_ref[...]).astype(BF16)
    value = mixed * active_ref[...]
    decays = jnp.exp(log_ref[...])
    row = lax.broadcasted_iota(jnp.int32, decays.shape, 0)
    factor = jnp.where(row == rows - 1, 1.0, pltpu.roll(decays, rows - 1, 0))
    inside = row % 8
    for step in (1, 2, 4):
        keep = inside + step < 8
        value_next = pltpu.roll(value, rows - step, 0)
        factor_next = pltpu.roll(factor, rows - step, 0)
        value = value + jnp.where(keep, factor * value_next, 0.0)
        factor = jnp.where(keep, factor * factor_next, factor)
    carry = jnp.zeros((1, decays.shape[1]), F32)
    span = jnp.ones((1, decays.shape[1]), F32)
    for block in range(rows // 8 - 1, -1, -1):
        at = slice(block * 8, block * 8 + 8)
        local = value[at] + factor[at] * carry
        spans = factor[at] * span
        local_out[at] = local
        span_out[at] = spans
        carry, span = local[:1], spans[:1]
    lead = decays[:1]
    edge_row = lax.broadcasted_iota(jnp.int32, edge_out.shape, 0)
    edge_out[...] = jnp.where(edge_row == 0, lead * span, lead * carry)


def recur(me, tokens, own, other, active, pull, log_decay):
    full = pltpu.VMEM(log_decay.shape, F32)
    return pl.pallas_call(
        recur_body,
        out_shape=[
            jax.ShapeDtypeStruct(log_decay.shape, BF16),
            full,
            full,
            pltpu.VMEM((8, log_decay.shape[1]), F32),
        ],
        in_specs=[pl.BlockSpec(memory_space=pltpu.SMEM)] + vmem_specs(6),
        out_specs=vmem_specs(4),
        compiler_params=room_for(8),
        name="recur",
    )(me, *kept_all([tokens, own, other, active, pull, log_decay]))


def finish_body(me_ref, own_ref, other_ref, local_ref, span_ref, past_ref, term_out, log_out):
    count = 2 * own_ref.shape[0]
    me = me_ref[0]

    def turn(i, carry):
        place = count - 1 - i
        relative = place ^ me
        mine, theirs = own_ref[relative // 2], other_ref[relative // 2]
        edge = jnp.where((relative & 1) == 0, mine, theirs)
        return jnp.where(place > me, edge[1:2] + edge[:1] * carry, carry)

    carry = lax.fori_loop(0, count - 1, turn, jnp.zeros((1, local_ref.shape[1]), F32))
    term = local_ref[...] + span_ref[...] * carry
    term_out[...] = term
    log_out[...] = (term * past_ref[...]).astype(BF16)


def finish(me, own, other, local, span, past):
    return pl.pallas_call(
        finish_body,
        out_shape=[
            jax.ShapeDtypeStruct(local.shape, F32),
            jax.ShapeDtypeStruct(local.shape, BF16),
        ],
        in_specs=[pl.BlockSpec(memory_space=pltpu.SMEM)] + vmem_specs(5),
        out_specs=vmem_specs(2),
        compiler_params=room_for(6),
        name="finish",
    )(me, *kept_all([own, other, local, span, past]))


def spread_body(me_ref, tokens_ref, *outs):
    for k, out in enumerate(outs):
        out[...] = tokens_ref[(me_ref[0] // 2) ^ k]


def spread(me, tokens):
    chips, rows, width = tokens.shape
    return pl.pallas_call(
        spread_body,
        out_shape=[pltpu.VMEM((rows, width), BF16)] * chips,
        in_specs=[pl.BlockSpec(memory_space=pltpu.SMEM)] + vmem_specs(1),
        out_specs=vmem_specs(chips),
        compiler_params=room_for(4),
        name="spread",
    )(me, kept(tokens))


def halves_body(me_ref, *refs):
    got, (own, other) = refs[:-2], refs[-2:]
    first = (me_ref[0] & 1) == 0
    half = own.shape[2]
    for k, piece in enumerate(got):
        left, right = piece[:, :half], piece[:, half:]
        own[k] = jnp.where(first, left, right)
        other[k] = jnp.where(first, right, left)


def halves(me, got):
    rows, width = got[0].shape
    return pl.pallas_call(
        halves_body,
        out_shape=[pltpu.VMEM((len(got), rows, width // 2), BF16)] * 2,
        in_specs=[pl.BlockSpec(memory_space=pltpu.SMEM)] + vmem_specs(len(got)),
        out_specs=vmem_specs(2),
        compiler_params=room_for(4),
        name="halves",
    )(me, *kept_all(got))


def proj_body(tok_own, tok_other, own_ref, other_ref, out):
    chips, rows, _ = tok_own.shape
    skip = own_ref.shape[1] - rows
    total = jnp.zeros(out.shape, F32)
    for k in range(chips):
        total += contract_rows(tok_own[k], own_ref[k, skip:])
    for k in range(chips):
        total += contract_rows(tok_other[k], other_ref[k, skip:])
    out[...] = total


def proj_grad(tok_own, tok_other, own, other):
    return pl.pallas_call(
        proj_body,
        out_shape=jax.ShapeDtypeStruct((tok_own.shape[2], own.shape[2]), F32),
        in_specs=vmem_specs(4),
        out_specs=vmem_specs(1)[0],
        compiler_params=room_for(6),
        name="proj_grad",
    )(*kept_all([tok_own, tok_other, own, other]))


def shards(
    moe_input,
    cotangent,
    routes,
    route_weights,
    gate_branch,
    log_decay,
    states,
    w_gate,
    w_up,
    w_down,
    out_proj,
):
    groups = lax.axis_size("sp")
    parts = lax.axis_size("tp")
    chips = groups // 2
    tok_rows, picks = routes.shape
    room = tok_rows * picks * 5 // (4 * groups)
    me = lax.axis_index("sp").astype(jnp.int32).reshape(1)
    order = lax.axis_index("tp").astype(jnp.int32) ^ jnp.arange(parts, dtype=jnp.int32)

    send_x, send_c, chosen = slots(
        me, routes.T, route_weights.T, moe_input, cotangent, groups, room
    )

    def between_chips(pieces):
        return [pieces[0]] + [swap(pieces[k], "sp", 2 * k) for k in range(1, chips)]

    def between_cores(got):
        other = swap(jnp.concatenate([piece[room:] for piece in got], axis=0), "sp", 1)
        return jnp.concatenate([piece[:room] for piece in got] + [other], axis=0)

    def between_parts(pieces):
        return [pieces[0]] + [swap(pieces[k], "tp", k) for k in range(1, parts)]

    got_x, got_c = between_chips(send_x), between_chips(send_c)
    earlier_state = lax.ppermute(
        states[-1:], "sp", [(source, source + 1) for source in range(groups - 1)]
    )
    past = jnp.exp(log_decay) * jnp.concatenate([earlier_state, states[:-1]], axis=0)
    active, pull, mixed_in = gates(gate_branch, states)
    bundle = jnp.concatenate([out_proj, mixed_in], axis=0)
    xs = between_parts([between_cores(got_x)] * parts)
    cs = between_parts([between_cores(got_c)] * parts)
    bundles = jnp.stack(between_chips([bundle] * chips))
    bundles_other = swap(bundles, "sp", 1)

    pre_gate, pre_up = forward(order, xs, w_gate, w_up)
    hidden, grad_gate, grad_up, terms = backward(
        order, cs, w_down, w_gate, w_up, pre_gate, pre_up
    )
    shares = between_parts(terms)
    grad_gate_w, grad_up_w, grad_down = weight_grads(
        order, xs, cs, hidden, grad_gate, grad_up
    )
    summed = sum(share.astype(F32) for share in shares).astype(BF16)

    near, far = summed[: chips * room], swap(summed[chips * room :], "sp", 1)
    spans = [slice(k * room, (k + 1) * room) for k in range(chips)]
    backs = [jnp.concatenate([near[at], far[at]], axis=0) for at in spans]
    backs = between_chips(backs)
    grad_cols = combine(chosen, cotangent, backs)
    tokens = lax.all_gather(grad_cols, "tp", axis=0)
    if parts != chips:
        model = parts * grad_cols.shape[1]
        tokens = tokens.transpose(1, 0, 2).reshape(tok_rows, chips, model // chips)
        tokens = tokens.transpose(1, 0, 2)

    got = between_chips(spread(me, tokens))
    grad_gate_branch, local, span, edge = recur(
        me, tokens, bundles, bundles_other, active, pull, log_decay
    )
    edges = jnp.stack(between_chips([edge] * chips))
    edges_other = swap(edges, "sp", 1)
    tok_own, tok_other = halves(me, got)
    tok_other = swap(tok_other, "sp", 1)
    grad_input_term, grad_log_decay = finish(me, edges, edges_other, local, span, past)
    grad_out_proj = proj_grad(tok_own, tok_other, bundles, bundles_other)
    return (
        grad_gate_w,
        grad_up_w,
        grad_down,
        grad_out_proj,
        grad_gate_branch,
        grad_log_decay,
        grad_input_term,
    )


def solution(mesh):
    return jax.shard_map(
        shards,
        mesh=mesh,
        in_specs=(
            P("sp", "tp"),
            P("sp", "tp"),
            P("sp", None),
            P("sp", None),
            P("sp", "tp"),
            P("sp", "tp"),
            P("sp", "tp"),
            P("sp", None, "tp"),
            P("sp", None, "tp"),
            P("sp", "tp", None),
            P("sp", "tp"),
        ),
        out_specs=(
            P("sp", None, "tp"),
            P("sp", None, "tp"),
            P("sp", "tp", None),
            P("sp", "tp"),
            P("sp", "tp"),
            P("sp", "tp"),
            P("sp", "tp"),
        ),
        check_vma=False,
    )
```

time: 256 us -> 171 us (0.67); the launches traced: 252 us -> 171 us
  local copies, waits for them, and re-layouts: 68.4 us -> 7.7 us
  blocking collectives: 69.8 us -> 10.1 us
  waiting for transfers between devices: 42.5 us -> 83.6 us
  starting transfers between devices: 7.14 us -> 42.3 us
  matrix products: 29.8 us -> 0 us
  Pallas kernels: 0 us -> 24.2 us
  other arithmetic: 18.7 us -> 2.06 us
  between operations: 15.9 us -> 0.97 us
    ppermute x1 -> x34, waiting for transfers between devices: 0.01 us -> 83.6 us  [the longest x33 83.6 us: swap(): return lax.ppermute(value, axis, [(i, i ^ bits) for i in range(count)])]
    slice x52 -> x11, local copies, waits for them, and re-layouts: 42.4 us -> 0.09 us  [the longest x7 0.05 us: between_cores(): piece[room:]]
    ppermute x1 -> x34, starting transfers between devices: 2.14 us -> 42.3 us  [the longest x33 41 us: swap(): return lax.ppermute(value, axis, [(i, i ^ bits) for i in range(count)])]
    all_gather x3 -> x0, waiting for transfers between devices: 34.3 us -> none  [the longest x1 24.9 us: shards(): lax.all_gather(part_cot, 'tp', axis=2, tiled=True)]
    all_to_all x2 -> x0, blocking collectives: 31.6 us -> none  [the longest x1 17.4 us: shards(): lax.all_to_all(send_data.reshape(groups, room, col_width), 'sp', split_ax...]
    dot_general x9 -> x0, matrix products: 29.8 us -> none  [the longest x4 15.8 us: contract_rows(): lax.dot_general(left_mat, right_mat, (((0,), (0,)), ((), ())), preferred_...]
    all_gather x3 -> x1, blocking collectives: 38.2 us -> 10.1 us  [shards(): tokens = lax.all_gather(grad_cols, 'tp', axis=0)]
    pallas_call x0 -> x11, Pallas kernels: none -> 24.2 us  [the longest x1 8.29 us: weight_grads(): pl.pallas_call(functools.partial(weights_body, parts), out_shape=[jax.Sha...]
  transfers between devices with their start and end apart: 7 -> 34, of which waited for: 4 -> 18; matrix products, arithmetic and copies ran while one was open for 40% -> 1% of each run, Pallas kernels for 0% -> 13%
where the time goes in v1:
time: 171 us
  waiting for transfers between devices  83.6 us (49%)
  starting transfers between devices  42.3 us (25%)
  Pallas kernels  24.2 us (14%)
  blocking collectives  10.1 us (6%)
  local copies, waits for them, and re-layouts  7.7 us (5%)
  other arithmetic  2.06 us (1%)
    ppermute x33, waiting for transfers between devices, swap(): return lax.ppermute(value, axis, [(i, i ^ bits) for i in range(count)])  83.6 us
    ppermute x33, starting transfers between devices, swap(): return lax.ppermute(value, axis, [(i, i ^ bits) for i in range(count)])  41 us
    all_gather x1, blocking collectives, shards(): tokens = lax.all_gather(grad_cols, 'tp', axis=0)  10.1 us
    pallas_call x1, Pallas kernels, weight_grads(): pl.pallas_call(functools.partial(weights_body, parts), out_shape=[jax.Sha...  8.29 us
    unnamed x33, local copies, waits for them, and re-layouts  7.56 us
    pallas_call x1, Pallas kernels, backward(): pl.pallas_call(functools.partial(backward_body, parts), out_shape=[pltpu....  3.71 us
  transfers between devices with their start and end apart: 34, of which 18 were waited for; matrix products, arithmetic and copies ran while one was open for 1% of the time, Pallas kernels for 13%

profile of v1, /device:TPU:0, one launch (start us, length us, event | category | flops | bytes accessed | tf_op | source)
XLA Modules:
  0.0 170.8 jit_solution(4220145482057530017)
XLA Ops:
  5.3 5.1 %collective-permute-start.27 = (bf16[384,640]{1,0:T(8,128)(2,1)S(1)}, bf16[384,640]{1,0:T(8,128)(2,1)S(1)}, u32[]{:S(2)}, u32[]{:S(2)}) collective-permute-start(bf16[384,640]{1,0:T(8,128)(2,1)S(1)} %constant_dynamic-update-slice_fusion.2), channel_id=1, source_target_pairs={{0,24},{4,28},{8,16},{12,20},{16,8},{20,12},{24,0},{28,4},{1,25},{... | collective-permute-start | bytes 1474568 | tf_op jit(solution)/shard_map/ppermute | solution.py:29
  14.6 30.9 %collective-permute-done.7 = bf16[80,512]{1,0:T(8,128)(2,1)S(1)} collective-permute-done((bf16[80,512]{1,0:T(8,128)(2,1)S(1)}, bf16[80,512]{1,0:T(8,128)(2,1)S(1)}, u32[]{:S(2)}, u32[]{:S(2)}) %collective-permute-start.7) | collective-permute-done | bytes 81952 | tf_op jit(solution)/shard_map/ppermute | solution.py:29
  46.9 3.6 %collective-permute-start.2 = (bf16[80,512]{1,0:T(8,128)(2,1)S(1)}, bf16[80,512]{1,0:T(8,128)(2,1)S(1)}, u32[]{:S(2)}, u32[]{:S(2)}) collective-permute-start(bf16[80,512]{1,0:T(8,128)(2,1)S(1)} %get-tuple-element.46), channel_id=1, source_target_pairs={{0,24},{4,28},{8,16},{12,20},{16,8},{20,12},{24,0},{28,4},{1,25},{... | collective-permute-start | bytes 245768 | tf_op jit(solution)/shard_map/ppermute | solution.py:29
  50.5 8.0 %collective-permute-done.1 = bf16[80,512]{1,0:T(8,128)(2,1)S(1)} collective-permute-done((bf16[80,512]{1,0:T(8,128)(2,1)S(1)}, bf16[80,512]{1,0:T(8,128)(2,1)S(1)}, u32[]{:S(2)}, u32[]{:S(2)}) %collective-permute-start.1) | collective-permute-done | bytes 81952 | tf_op jit(solution)/shard_map/ppermute | solution.py:29
  58.6 2.5 %collective-permute-start.9 = (bf16[80,512]{1,0:T(8,128)(2,1)S(1)}, bf16[80,512]{1,0:T(8,128)(2,1)S(1)}, u32[]{:S(2)}, u32[]{:S(2)}) collective-permute-start(bf16[80,512]{1,0:T(8,128)(2,1)S(1)} %get-tuple-element.50), channel_id=1, source_target_pairs={{0,24},{4,28},{8,16},{12,20},{16,8},{20,12},{24,0},{28,4},{1,25},{... | collective-permute-start | bytes 245768 | tf_op jit(solution)/shard_map/ppermute | solution.py:29
  61.1 4.9 %collective-permute-done.8 = bf16[80,512]{1,0:T(8,128)(2,1)S(1)} collective-permute-done((bf16[80,512]{1,0:T(8,128)(2,1)S(1)}, bf16[80,512]{1,0:T(8,128)(2,1)S(1)}, u32[]{:S(2)}, u32[]{:S(2)}) %collective-permute-start.8) | collective-permute-done | bytes 81952 | tf_op jit(solution)/shard_map/ppermute | solution.py:29
  67.5 2.5 %collective-permute-start.6 = (bf16[320,512]{1,0:T(8,128)(2,1)S(1)}, bf16[320,512]{1,0:T(8,128)(2,1)S(1)}, u32[]{:S(2)}, u32[]{:S(2)}) collective-permute-start(bf16[320,512]{1,0:T(8,128)(2,1)S(1)} %constant_dynamic-update-slice_fusion.refs_0_), channel_id=1, source_target_pairs={{0,3},{1,2},{2,1},{3,0},{4,7},{5,6},{6,5},{7,4},{8,11},{9,10},{10,... | collective-permute-start | bytes 983048 | tf_op jit(solution)/shard_map/ppermute | solution.py:29
  72.6 2.4 %collective-permute-start.13 = (bf16[320,512]{1,0:T(8,128)(2,1)S(1)}, bf16[320,512]{1,0:T(8,128)(2,1)}, u32[]{:S(2)}, u32[]{:S(2)}) collective-permute-start(bf16[320,512]{1,0:T(8,128)(2,1)S(1)} %constant_dynamic-update-slice_fusion.1.refs_0_.refs_4_), channel_id=1, source_target_pairs={{0,3},{1,2},{2,1},{3,0},{4,7},{5,6},{6,5},{7,4},{8,11},{9,10},{10,... | collective-permute-start | bytes 983048 | tf_op jit(solution)/shard_map/ppermute | solution.py:29
  75.6 3.5 %collective-permute-done.6.refs_3_ = bf16[320,512]{1,0:T(8,128)(2,1)S(1)} collective-permute-done((bf16[320,512]{1,0:T(8,128)(2,1)S(1)}, bf16[320,512]{1,0:T(8,128)(2,1)S(1)}, u32[]{:S(2)}, u32[]{:S(2)}) %collective-permute-start.6) | collective-permute-done | bytes 327712 | tf_op jit(solution)/shard_map/ppermute | solution.py:29
  82.3 3.8 %collective-permute-done.5.refs_2_ = bf16[320,512]{1,0:T(8,128)(2,1)S(1)} collective-permute-done((bf16[320,512]{1,0:T(8,128)(2,1)S(1)}, bf16[320,512]{1,0:T(8,128)(2,1)S(1)}, u32[]{:S(2)}, u32[]{:S(2)}) %collective-permute-start.5) | collective-permute-done | bytes 327712 | tf_op jit(solution)/shard_map/ppermute | solution.py:29
  89.4 2.6 %expert_forward.1 = (f32[320,512]{1,0:T(8,128)S(1)}, f32[320,512]{1,0:T(8,128)S(1)}) custom-call(s32[4]{0:T(128)S(1)} %iota_xor_fusion.order_ref, bf16[320,512]{1,0:T(8,128)(2,1)S(1)} %constant_dynamic-update-slice_fusion.refs_0_, bf16[320,512]{1,0:T(8,128)(2,1)} %collective-permute-done.4.refs_1_, bf16[320,512]{1,0:T(8,128)(2,1)S(1)} %collective-permute-done.5.refs_2_, ...), custom_call_target="tpu_custom_call" | custom-call | tf_op jit(solution)/shard_map/expert_forward/pallas_call | solution.py:115
  93.2 6.1 %collective-permute-done.12.refs_2_.refs_6_ = bf16[320,512]{1,0:T(8,128)(2,1)} collective-permute-done((bf16[320,512]{1,0:T(8,128)(2,1)S(1)}, bf16[320,512]{1,0:T(8,128)(2,1)}, u32[]{:S(2)}, u32[]{:S(2)}) %collective-permute-start.12) | collective-permute-done | bytes 327712 | tf_op jit(solution)/shard_map/ppermute | solution.py:29
  99.5 3.7 %expert_backward.1 = (bf16[320,512]{1,0:T(8,128)(2,1)S(1)}, bf16[320,512]{1,0:T(8,128)(2,1)S(1)}, bf16[320,512]{1,0:T(8,128)(2,1)S(1)}, bf16[320,512]{1,0:T(8,12...) custom-call(s32[4]{0:T(128)S(1)} %iota_xor_fusion.order_ref, ...), custom_call_target="tpu_custom_call" | custom-call | tf_op jit(solution)/shard_map/expert_backward/pallas_call | solution.py:155
  106.8 7.1 %collective-permute-done.14 = bf16[320,512]{1,0:T(8,128)(2,1)S(1)} collective-permute-done((bf16[320,512]{1,0:T(8,128)(2,1)S(1)}, bf16[320,512]{1,0:T(8,128)(2,1)S(1)}, u32[]{:S(2)}, u32[]{:S(2)}) %collective-permute-start.14) | collective-permute-done | bytes 327712 | tf_op jit(solution)/shard_map/ppermute | solution.py:29
  113.9 7.2 %collective-permute-done.15 = bf16[320,512]{1,0:T(8,128)(2,1)S(1)} collective-permute-done((bf16[320,512]{1,0:T(8,128)(2,1)S(1)}, bf16[320,512]{1,0:T(8,128)(2,1)S(1)}, u32[]{:S(2)}, u32[]{:S(2)}) %collective-permute-start.15) | collective-permute-done | bytes 327712 | tf_op jit(solution)/shard_map/ppermute | solution.py:29
  122.9 2.5 %collective-permute-start.19 = (bf16[80,512]{1,0:T(8,128)(2,1)S(1)}, bf16[80,512]{1,0:T(8,128)(2,1)S(1)}, u32[]{:S(2)}, u32[]{:S(2)}) collective-permute-start(bf16[80,512]{1,0:T(8,128)(2,1)S(1)} %pad_maximum_fusion.5), channel_id=1, source_target_pairs={{0,16},{4,20},{8,24},{12,28},{16,0},{20,4},{24,8},{28,12},{1,17},{... | collective-permute-start | bytes 245768 | tf_op jit(solution)/shard_map/ppermute | solution.py:29
  128.4 4.3 %collective-permute-done.19.refs_2_ = bf16[80,512]{1,0:T(8,128)(2,1)S(1)} collective-permute-done((bf16[80,512]{1,0:T(8,128)(2,1)S(1)}, bf16[80,512]{1,0:T(8,128)(2,1)S(1)}, u32[]{:S(2)}, u32[]{:S(2)}) %collective-permute-start.19) | collective-permute-done | bytes 81952 | tf_op jit(solution)/shard_map/ppermute | solution.py:29
  133.0 10.1 %all-gather = bf16[512,512]{1,0:T(8,128)(2,1)S(1)} all-gather(bf16[128,512]{1,0:T(8,128)(2,1)S(1)} %combine.1), channel_id=2, replica_groups=mesh['sp'=8,'tp'=4] {'tp'}, dimensions={0}, use_global_device_ids=true | all-gather | bytes 655360 | tf_op jit(solution)/shard_map/all_gather | solution.py:461
  143.1 2.0 %collective-permute-start.21 = (bf16[128,512]{1,0:T(8,128)(2,1)S(1)}, bf16[128,512]{1,0:T(8,128)(2,1)S(1)}, u32[]{:S(2)}, u32[]{:S(2)}) collective-permute-start(bf16[128,512]{1,0:T(8,128)(2,1)S(1)} %get-tuple-element.65), channel_id=1, source_target_pairs={{0,8},{4,12},{8,0},{12,4},{16,24},{20,28},{24,16},{28,20},{1,9},{5... | collective-permute-start | bytes 393224 | tf_op jit(solution)/shard_map/ppermute | solution.py:29
  147.6 3.2 %recur.1 = (bf16[128,640]{1,0:T(8,128)(2,1)}, f32[128,640]{1,0:T(8,128)S(1)}, f32[128,640]{1,0:T(8,128)S(1)}, f32[8,640]{1,0:T(8,128)S(1)}) custom-call(s32[1]{0:T(128)} %bitcast.me_ref, bf16[4,128,512]{2,1,0:T(8,128)(2,1)S(1)} %bitcast.14, bf16[4,384,640]{2,1,0:T(8,128)(2,1)S(1)} %pad_maximum_fusion.own_ref, ...), custom_call_target="tpu_custom_call" | custom-call | tf_op jit(solution)/shard_map/recur/pallas_call | solution.py:292
  150.8 2.0 %collective-permute-start.31 = (f32[8,640]{1,0:T(8,128)S(1)}, f32[8,640]{1,0:T(8,128)S(1)}, u32[]{:S(2)}, u32[]{:S(2)}) collective-permute-start(f32[8,640]{1,0:T(8,128)S(1)} %get-tuple-element.74), channel_id=1, source_target_pairs={{0,24},{4,28},{8,16},{12,20},{16,8},{20,12},{24,0},{28,4},{1,25},{... | collective-permute-start | bytes 61448 | tf_op jit(solution)/shard_map/ppermute | solution.py:29
  153.3 1.9 %collective-permute-start.29 = (f32[8,640]{1,0:T(8,128)S(1)}, f32[8,640]{1,0:T(8,128)S(1)}, u32[]{:S(2)}, u32[]{:S(2)}) collective-permute-start(f32[8,640]{1,0:T(8,128)S(1)} %get-tuple-element.74), channel_id=1, source_target_pairs={{0,8},{4,12},{8,0},{12,4},{16,24},{20,28},{24,16},{28,20},{1,9},{5... | collective-permute-start | bytes 61448 | tf_op jit(solution)/shard_map/ppermute | solution.py:29
  158.3 8.3 %weight_grads.1 = (f32[1,2048,512]{2,1,0:T(8,128)}, f32[1,2048,512]{2,1,0:T(8,128)}, f32[1,512,2048]{2,1,0:T(8,128)}) custom-call(s32[4]{0:T(128)S(1)} %iota_xor_fusion.order_ref, bf16[320,512]{1,0:T(8,128)(2,1)S(1)} %constant_dynamic-update-slice_fusion.refs_0_, bf16[320,512]{1,0:T(8,128)(2,1)} %collective-permute-done.4.refs_1_, ...), custom_call_target="tpu_custom_call" | custom-call | tf_op jit(solution)/shard_map/weight_grads/pallas_call | solution.py:188
  166.6 3.2 %proj_grad.1 = f32[256,640]{1,0:T(8,128)} custom-call(bf16[4,128,256]{2,1,0:T(8,128)(2,1)S(1)} %get-tuple-element.68.tok_own, bf16[4,128,256]{2,1,0:T(8,128)(2,1)S(1)} %collective-permute-done.24.tok_other, bf16[4,384,640]{2,1,0:T(8,128)(2,1)S(1)} %pad_maximum_fusion.own_ref, bf16[4,384,640]{2,1,0:T(8,128)(2,1)} %collective-permute-done.28.other_ref), custom_call_target="tpu_custom_call" | custom-call | tf_op jit(solution)/shard_map/proj_grad/pallas_call | solution.py:389
  (114 shorter events, 38.2 us)
Async XLA Ops:
  5.3 66.7 %collective-permute-start.27 = (bf16[384,640]{1,0:T(8,128)(2,1)S(1)}, bf16[384,640]{1,0:T(8,128)(2,1)S(1)}, u32[]{:S(2)}, u32[]{:S(2)}) collective-permute-start(bf16[384,640]{1,0:T(8,128)(2,1)S(1)} %constant_dynamic-update-slice_fusion.2), channel_id=1, source_target_pairs={{0,24},{4,28},{8,16},{12,20},{16,8},{20,12},{24,0},{28,4},{1,25},{... | collective-permute-start | bytes 1474568 | tf_op jit(solution)/shard_map/ppermute | solution.py:29
  10.4 62.2 %collective-permute-start.26 = (bf16[384,640]{1,0:T(8,128)(2,1)S(1)}, bf16[384,640]{1,0:T(8,128)(2,1)S(1)}, u32[]{:S(2)}, u32[]{:S(2)}) collective-permute-start(bf16[384,640]{1,0:T(8,128)(2,1)S(1)} %constant_dynamic-update-slice_fusion.2), channel_id=1, source_target_pairs={{0,16},{4,20},{8,24},{12,28},{16,0},{20,4},{24,8},{28,12},{1,17},{... | collective-permute-start | bytes 1474568 | tf_op jit(solution)/shard_map/ppermute | solution.py:29
  10.4 64.6 %collective-permute-start.25 = (bf16[384,640]{1,0:T(8,128)(2,1)S(1)}, bf16[384,640]{1,0:T(8,128)(2,1)}, u32[]{:S(2)}, u32[]{:S(2)}) collective-permute-start(bf16[384,640]{1,0:T(8,128)(2,1)S(1)} %constant_dynamic-update-slice_fusion.2), channel_id=1, source_target_pairs={{0,8},{4,12},{8,0},{12,4},{16,24},{20,28},{24,16},{28,20},{1,9},{5... | collective-permute-start | bytes 1474568 | tf_op jit(solution)/shard_map/ppermute | solution.py:29
  12.5 34.4 %collective-permute-start = (bf16[80,512]{1,0:T(8,128)(2,1)S(1)}, bf16[80,512]{1,0:T(8,128)(2,1)S(1)}, u32[]{:S(2)}, u32[]{:S(2)}) collective-permute-start(bf16[80,512]{1,0:T(8,128)(2,1)S(1)} %get-tuple-element.44), channel_id=1, source_target_pairs={{0,8},{4,12},{8,0},{12,4},{16,24},{20,28},{24,16},{28,20},{1,9},{5... | collective-permute-start | bytes 245768 | tf_op jit(solution)/shard_map/ppermute | solution.py:29
  14.0 31.6 %collective-permute-start.7 = (bf16[80,512]{1,0:T(8,128)(2,1)S(1)}, bf16[80,512]{1,0:T(8,128)(2,1)S(1)}, u32[]{:S(2)}, u32[]{:S(2)}) collective-permute-start(bf16[80,512]{1,0:T(8,128)(2,1)S(1)} %get-tuple-element.48), channel_id=1, source_target_pairs={{0,8},{4,12},{8,0},{12,4},{16,24},{20,28},{24,16},{28,20},{1,9},{5... | collective-permute-start | bytes 245768 | tf_op jit(solution)/shard_map/ppermute | solution.py:29
  45.6 13.0 %collective-permute-start.1 = (bf16[80,512]{1,0:T(8,128)(2,1)S(1)}, bf16[80,512]{1,0:T(8,128)(2,1)S(1)}, u32[]{:S(2)}, u32[]{:S(2)}) collective-permute-start(bf16[80,512]{1,0:T(8,128)(2,1)S(1)} %get-tuple-element.45), channel_id=1, source_target_pairs={{0,16},{4,20},{8,24},{12,28},{16,0},{20,4},{24,8},{28,12},{1,17},{... | collective-permute-start | bytes 245768 | tf_op jit(solution)/shard_map/ppermute | solution.py:29
  46.9 11.7 %collective-permute-start.2 = (bf16[80,512]{1,0:T(8,128)(2,1)S(1)}, bf16[80,512]{1,0:T(8,128)(2,1)S(1)}, u32[]{:S(2)}, u32[]{:S(2)}) collective-permute-start(bf16[80,512]{1,0:T(8,128)(2,1)S(1)} %get-tuple-element.46), channel_id=1, source_target_pairs={{0,24},{4,28},{8,16},{12,20},{16,8},{20,12},{24,0},{28,4},{1,25},{... | collective-permute-start | bytes 245768 | tf_op jit(solution)/shard_map/ppermute | solution.py:29
  58.5 7.5 %collective-permute-start.8 = (bf16[80,512]{1,0:T(8,128)(2,1)S(1)}, bf16[80,512]{1,0:T(8,128)(2,1)S(1)}, u32[]{:S(2)}, u32[]{:S(2)}) collective-permute-start(bf16[80,512]{1,0:T(8,128)(2,1)S(1)} %get-tuple-element.49), channel_id=1, source_target_pairs={{0,16},{4,20},{8,24},{12,28},{16,0},{20,4},{24,8},{28,12},{1,17},{... | collective-permute-start | bytes 245768 | tf_op jit(solution)/shard_map/ppermute | solution.py:29
  67.5 11.6 %collective-permute-start.6 = (bf16[320,512]{1,0:T(8,128)(2,1)S(1)}, bf16[320,512]{1,0:T(8,128)(2,1)S(1)}, u32[]{:S(2)}, u32[]{:S(2)}) collective-permute-start(bf16[320,512]{1,0:T(8,128)(2,1)S(1)} %constant_dynamic-update-slice_fusion.refs_0_), channel_id=1, source_target_pairs={{0,3},{1,2},{2,1},{3,0},{4,7},{5,6},{6,5},{7,4},{8,11},{9,10},{10,... | collective-permute-start | bytes 983048 | tf_op jit(solution)/shard_map/ppermute | solution.py:29
  71.5 14.7 %collective-permute-start.5 = (bf16[320,512]{1,0:T(8,128)(2,1)S(1)}, bf16[320,512]{1,0:T(8,128)(2,1)S(1)}, u32[]{:S(2)}, u32[]{:S(2)}) collective-permute-start(bf16[320,512]{1,0:T(8,128)(2,1)S(1)} %constant_dynamic-update-slice_fusion.refs_0_), channel_id=1, source_target_pairs={{0,2},{1,3},{2,0},{3,1},{4,6},{5,7},{6,4},{7,5},{8,10},{9,11},{10,... | collective-permute-start | bytes 983048 | tf_op jit(solution)/shard_map/ppermute | solution.py:29
  72.0 14.2 %collective-permute-start.4 = (bf16[320,512]{1,0:T(8,128)(2,1)S(1)}, bf16[320,512]{1,0:T(8,128)(2,1)}, u32[]{:S(2)}, u32[]{:S(2)}) collective-permute-start(bf16[320,512]{1,0:T(8,128)(2,1)S(1)} %constant_dynamic-update-slice_fusion.refs_0_), channel_id=1, source_target_pairs={{0,1},{1,0},{2,3},{3,2},{4,5},{5,4},{6,7},{7,6},{8,9},{9,8},{10,11... | collective-permute-start | bytes 983048 | tf_op jit(solution)/shard_map/ppermute | solution.py:29
  72.6 20.6 %collective-permute-start.13 = (bf16[320,512]{1,0:T(8,128)(2,1)S(1)}, bf16[320,512]{1,0:T(8,128)(2,1)}, u32[]{:S(2)}, u32[]{:S(2)}) collective-permute-start(bf16[320,512]{1,0:T(8,128)(2,1)S(1)} %constant_dynamic-update-slice_fusion.1.refs_0_.refs_4_), channel_id=1, source_target_pairs={{0,3},{1,2},{2,1},{3,0},{4,7},{5,6},{6,5},{7,4},{8,11},{9,10},{10,... | collective-permute-start | bytes 983048 | tf_op jit(solution)/shard_map/ppermute | solution.py:29
  75.1 24.3 %collective-permute-start.12 = (bf16[320,512]{1,0:T(8,128)(2,1)S(1)}, bf16[320,512]{1,0:T(8,128)(2,1)}, u32[]{:S(2)}, u32[]{:S(2)}) collective-permute-start(bf16[320,512]{1,0:T(8,128)(2,1)S(1)} %constant_dynamic-update-slice_fusion.1.refs_0_.refs_4_), channel_id=1, source_target_pairs={{0,2},{1,3},{2,0},{3,1},{4,6},{5,7},{6,4},{7,5},{8,10},{9,11},{10,... | collective-permute-start | bytes 983048 | tf_op jit(solution)/shard_map/ppermute | solution.py:29
  79.1 20.4 %collective-permute-start.11 = (bf16[320,512]{1,0:T(8,128)(2,1)S(1)}, bf16[320,512]{1,0:T(8,128)(2,1)}, u32[]{:S(2)}, u32[]{:S(2)}) collective-permute-start(bf16[320,512]{1,0:T(8,128)(2,1)S(1)} %constant_dynamic-update-slice_fusion.1.refs_0_.refs_4_), channel_id=1, source_target_pairs={{0,1},{1,0},{2,3},{3,2},{4,5},{5,4},{6,7},{7,6},{8,9},{9,8},{10,11... | collective-permute-start | bytes 983048 | tf_op jit(solution)/shard_map/ppermute | solution.py:29
  86.1 61.5 %collective-permute-start.28 = (bf16[4,384,640]{2,1,0:T(8,128)(2,1)S(1)}, bf16[4,384,640]{2,1,0:T(8,128)(2,1)}, u32[]{:S(2)}, u32[]{:S(2)}) collective-permute-start(bf16[4,384,640]{2,1,0:T(8,128)(2,1)S(1)} %pad_maximum_fusion.own_ref), channel_id=1, source_target_pairs={{0,4},{4,0},{8,12},{12,8},{16,20},{20,16},{24,28},{28,24},{1,5},{5... | collective-permute-start | bytes 5898248 | tf_op jit(solution)/shard_map/ppermute | solution.py:29
  103.2 10.6 %collective-permute-start.14 = (bf16[320,512]{1,0:T(8,128)(2,1)S(1)}, bf16[320,512]{1,0:T(8,128)(2,1)S(1)}, u32[]{:S(2)}, u32[]{:S(2)}) collective-permute-start(bf16[320,512]{1,0:T(8,128)(2,1)S(1)} %get-tuple-element.61), channel_id=1, source_target_pairs={{0,1},{1,0},{2,3},{3,2},{4,5},{5,4},{6,7},{7,6},{8,9},{9,8},{10,11... | collective-permute-start | bytes 983048 | tf_op jit(solution)/shard_map/ppermute | solution.py:29
  104.8 16.3 %collective-permute-start.15 = (bf16[320,512]{1,0:T(8,128)(2,1)S(1)}, bf16[320,512]{1,0:T(8,128)(2,1)S(1)}, u32[]{:S(2)}, u32[]{:S(2)}) collective-permute-start(bf16[320,512]{1,0:T(8,128)(2,1)S(1)} %get-tuple-element.62), channel_id=1, source_target_pairs={{0,2},{1,3},{2,0},{3,1},{4,6},{5,7},{6,4},{7,5},{8,10},{9,11},{10,... | collective-permute-start | bytes 983048 | tf_op jit(solution)/shard_map/ppermute | solution.py:29
  106.2 14.9 %collective-permute-start.16 = (bf16[320,512]{1,0:T(8,128)(2,1)S(1)}, bf16[320,512]{1,0:T(8,128)(2,1)S(1)}, u32[]{:S(2)}, u32[]{:S(2)}) collective-permute-start(bf16[320,512]{1,0:T(8,128)(2,1)S(1)} %get-tuple-element.63), channel_id=1, source_target_pairs={{0,3},{1,2},{2,1},{3,0},{4,7},{5,6},{6,5},{7,4},{8,11},{9,10},{10,... | collective-permute-start | bytes 983048 | tf_op jit(solution)/shard_map/ppermute | solution.py:29
  122.9 9.8 %collective-permute-start.19 = (bf16[80,512]{1,0:T(8,128)(2,1)S(1)}, bf16[80,512]{1,0:T(8,128)(2,1)S(1)}, u32[]{:S(2)}, u32[]{:S(2)}) collective-permute-start(bf16[80,512]{1,0:T(8,128)(2,1)S(1)} %pad_maximum_fusion.5), channel_id=1, source_target_pairs={{0,16},{4,20},{8,24},{12,28},{16,0},{20,4},{24,8},{28,12},{1,17},{... | collective-permute-start | bytes 245768 | tf_op jit(solution)/shard_map/ppermute | solution.py:29
  143.1 10.2 %collective-permute-start.21 = (bf16[128,512]{1,0:T(8,128)(2,1)S(1)}, bf16[128,512]{1,0:T(8,128)(2,1)S(1)}, u32[]{:S(2)}, u32[]{:S(2)}) collective-permute-start(bf16[128,512]{1,0:T(8,128)(2,1)S(1)} %get-tuple-element.65), channel_id=1, source_target_pairs={{0,8},{4,12},{8,0},{12,4},{16,24},{20,28},{24,16},{28,20},{1,9},{5... | collective-permute-start | bytes 393224 | tf_op jit(solution)/shard_map/ppermute | solution.py:29
  145.1 10.5 %collective-permute-start.22 = (bf16[128,512]{1,0:T(8,128)(2,1)S(1)}, bf16[128,512]{1,0:T(8,128)(2,1)S(1)}, u32[]{:S(2)}, u32[]{:S(2)}) collective-permute-start(bf16[128,512]{1,0:T(8,128)(2,1)S(1)} %get-tuple-element.66), channel_id=1, source_target_pairs={{0,16},{4,20},{8,24},{12,28},{16,0},{20,4},{24,8},{28,12},{1,17},{... | collective-permute-start | bytes 393224 | tf_op jit(solution)/shard_map/ppermute | solution.py:29
  145.7 11.2 %collective-permute-start.23 = (bf16[128,512]{1,0:T(8,128)(2,1)S(1)}, bf16[128,512]{1,0:T(8,128)(2,1)S(1)}, u32[]{:S(2)}, u32[]{:S(2)}) collective-permute-start(bf16[128,512]{1,0:T(8,128)(2,1)S(1)} %get-tuple-element.67), channel_id=1, source_target_pairs={{0,24},{4,28},{8,16},{12,20},{16,8},{20,12},{24,0},{28,4},{1,25},{... | collective-permute-start | bytes 393224 | tf_op jit(solution)/shard_map/ppermute | solution.py:29
  157.0 9.6 %collective-permute-start.24 = (bf16[4,128,256]{2,1,0:T(8,128)(2,1)S(1)}, bf16[4,128,256]{2,1,0:T(8,128)(2,1)S(1)}, u32[]{:S(2)}, u32[]{:S(2)}) collective-permute-start(bf16[4,128,256]{2,1,0:T(8,128)(2,1)S(1)} %get-tuple-element.69), channel_id=1, source_target_pairs={{0,4},{4,0},{8,12},{12,8},{16,20},{20,16},{24,28},{28,24},{1,5},{5... | collective-permute-start | bytes 786440 | tf_op jit(solution)/shard_map/ppermute | solution.py:29
  158.2 11.7 %collective-permute-start.32 = (f32[4,8,640]{2,1,0:T(8,128)S(1)}, f32[4,8,640]{2,1,0:T(8,128)S(1)}, u32[]{:S(2)}, u32[]{:S(2)}) collective-permute-start(f32[4,8,640]{2,1,0:T(8,128)S(1)} %pad_maximum_fusion.7.own_ref), channel_id=1, source_target_pairs={{0,4},{4,0},{8,12},{12,8},{16,20},{20,16},{24,28},{28,24},{1,5},{5... | collective-permute-start | bytes 245768 | tf_op jit(solution)/shard_map/ppermute | solution.py:29
  (26 other events, 278.8 us)
